TPU v7x, 32 devices: a whole 2x2x4 slice. The times are simulated.
32 devices in a mesh: sp: 8 (over z, y), tp: 4 (over x, core).
Axes of the slice: x: 2, y: 2, z: 4, core: 2. Of those that a mesh axis runs over, the one named last changes fastest.
Arguments:
- queries: bfloat16 [2048, 2048], P('sp', 'tp'), may hold values from -6 to 6
- keys: bfloat16 [2048, 512], P('sp', 'tp'), may hold values from -6 to 6
- values: bfloat16 [2048, 512], P('sp', 'tp'), may hold values from -6 to 6
- query_gain: float32 [64], replicated, may hold values from 0.8 to 5
- key_gain: float32 [64], replicated, may hold values from 0.8 to 5
- stream: bfloat16 [2048, 2048], P('sp'), may hold values from -0.1796875 to 0.1796875
- out_weight: bfloat16 [2048, 2048], P('tp'), may hold values from -0.125 to 0.125
- mixer_gain: float32 [2048], replicated, may hold values from 0.1 to 1.9
- up_weight: bfloat16 [2048, 8192], P('sp', 'tp'), may hold values from -0.125 to 0.125
- down_weight: bfloat16 [8192, 2048], P('tp', 'sp'), may hold values from -0.0625 to 0.0625
Outputs:
- updated: bfloat16 [2048, 2048], P('sp', 'tp')
All inputs are finite; a program needn't handle non-finite values.
Results may differ from a plain program's by a relative error of at most 0.02.
The roundings to bfloat16 on the way count: a program that leaves them out, or rounds other values in their place, can miss the bound.
Values may be sent and summed in bfloat16 or wider, within the bound.
A program may use at most 128 MiB of HBM per device.

v0:
```python
import math

import jax
import jax.numpy as jnp
from jax import lax
from jax.sharding import PartitionSpec as P

HD = 64
GRID_W = 64


EPSILON = 1e-06


def prepare(projected, gain_vec, offset):
    row_count = projected.shape[0]
    head_count = projected.shape[1] // HD
    widened = projected.astype(jnp.float32).reshape(row_count, head_count, HD)
    widened = (
        widened
        * lax.rsqrt(jnp.mean(widened * widened, axis=-1, keepdims=True) + EPSILON)
        * gain_vec
    )
    position = offset + jnp.arange(row_count, dtype=jnp.int32)
    grid_row = (position // GRID_W).astype(jnp.float32)
    grid_col = (position % GRID_W).astype(jnp.float32)
    half_dim = HD // 2
    inverse = 1.0 / jnp.power(10000.0, jnp.arange(0, half_dim, 2, dtype=jnp.float32) / half_dim)
    angle = jnp.concatenate([grid_row[:, None] * inverse, grid_col[:, None] * inverse], axis=-1)
    cosine = jnp.cos(angle)[:, None, :]
    sine_table = jnp.sin(angle)[:, None, :]
    paired = widened.reshape(row_count, head_count, half_dim, 2)
    former = paired[..., 0]
    latter = paired[..., 1]
    rotated = jnp.stack(
        [former * cosine - latter * sine_table, former * sine_table + latter * cosine], axis=-1
    )
    return rotated.reshape(row_count, head_count, HD).astype(jnp.bfloat16)


def attend_block(state, grouped, key_block, value_block):
    running, totals, weighted = state
    scores = jnp.einsum("qhgd,khd->hgqk", grouped, key_block, preferred_element_type=jnp.float32)
    scores = scores * (1.0 / math.sqrt(HD))
    newest = jnp.maximum(running, jnp.max(scores, axis=-1))
    rescale = jnp.exp(running - newest)
    exps = jnp.exp(scores - newest[..., None])
    totals = totals * rescale + jnp.sum(exps, axis=-1)
    weighted = weighted * rescale[..., None] + jnp.einsum(
        "hgqk,khd->hgqd", exps.astype(jnp.bfloat16), value_block, preferred_element_type=jnp.float32
    )
    return (newest, totals, weighted)


def shards(
    queries,
    keys,
    values,
    query_gain,
    key_gain,
    stream,
    out_weight,
    mixer_gain,
    up_weight,
    down_weight,
):
    local_rows = queries.shape[0]
    offset = lax.axis_index("sp") * local_rows
    kv_count = keys.shape[1] // HD
    group_size = queries.shape[1] // HD // kv_count
    grouped = prepare(queries, query_gain, offset).reshape(local_rows, kv_count, group_size, HD)
    prepared_keys = prepare(keys, key_gain, offset).reshape(local_rows, kv_count * HD)
    initial = (
        jnp.full((kv_count, group_size, local_rows), -1e30, jnp.float32),
        jnp.zeros((kv_count, group_size, local_rows), jnp.float32),
        jnp.zeros((kv_count, group_size, local_rows, HD), jnp.float32),
    )
    key_rows = lax.all_gather(prepared_keys, "sp", axis=0, tiled=True)
    value_rows = lax.all_gather(values, "sp", axis=0, tiled=True)
    piece_rows = key_rows.shape[0]
    block_rows = piece_rows if piece_rows <= 2048 else math.gcd(piece_rows, 2048)
    key_blocks = key_rows.reshape(piece_rows // block_rows, block_rows, kv_count, HD)
    value_blocks = value_rows.reshape(piece_rows // block_rows, block_rows, kv_count, HD)

    def visit_block(block_index, state_now):
        return attend_block(state_now, grouped, key_blocks[block_index], value_blocks[block_index])

    running, totals, weighted = lax.fori_loop(0, piece_rows // block_rows, visit_block, initial)
    head_out = weighted / totals[..., None]
    head_out = jnp.transpose(head_out, (2, 0, 1, 3)).reshape(local_rows, -1).astype(jnp.bfloat16)
    partial_value = jnp.dot(head_out, out_weight, preferred_element_type=jnp.float32)
    model_width = partial_value.shape[1]
    share_cols = model_width // lax.axis_size("tp")
    first_col = lax.axis_index("tp") * share_cols
    summed = lax.psum(partial_value.astype(jnp.bfloat16), "tp").astype(jnp.float32)
    mid = (stream.astype(jnp.float32) + summed).astype(jnp.bfloat16)
    mid_wide = mid.astype(jnp.float32)
    normed = (
        mid_wide
        * lax.rsqrt(jnp.mean(mid_wide * mid_wide, axis=-1, keepdims=True) + EPSILON)
        * mixer_gain
    )
    normed = normed.astype(jnp.bfloat16)
    own_mid = lax.dynamic_slice_in_dim(mid, first_col, share_cols, 1)
    up_sums = jnp.dot(
        normed,
        lax.all_gather(up_weight, "sp", axis=0, tiled=True),
        preferred_element_type=jnp.float32,
    )
    hidden = jnp.square(jax.nn.relu(up_sums)).astype(jnp.bfloat16)
    down_part = jnp.dot(
        hidden,
        lax.all_gather(down_weight, "sp", axis=1, tiled=True),
        preferred_element_type=jnp.float32,
    )
    down_share = lax.psum_scatter(
        down_part.astype(jnp.bfloat16), "tp", scatter_dimension=1, tiled=True
    ).astype(jnp.float32)
    return (own_mid.astype(jnp.float32) + down_share).astype(jnp.bfloat16)


def solution(mesh):
    return jax.shard_map(
        shards,
        mesh=mesh,
        in_specs=(
            P("sp", "tp"),
            P("sp", "tp"),
            P("sp", "tp"),
            P(),
            P(),
            P("sp", None),
            P("tp", None),
            P(),
            P("sp", "tp"),
            P("tp", "sp"),
        ),
        out_specs=P("sp", "tp"),
        check_vma=False,
    )
```

profile of v0, /device:TPU:0, one launch (start us, length us, event | category | flops | bytes accessed | tf_op | source)
XLA Modules:
  0.0 400.8 jit_solution(354414603991874629)
XLA Ops:
  7.4 0.0 copy-start
  7.4 0.0 all-reduce.2.cloned.1.call-start
  7.4 1.2 copy.18
  8.6 0.3 reshape.165
  8.9 0.1 bitcast_reduce_fusion.1
  9.0 0.9 copy.17
  9.9 0.1 reshape.164
  10.1 0.8 mul.244
  10.8 0.1 broadcast_multiply_fusion.1
  10.9 0.1 fusion.28
  11.0 0.3 multiply_multiply_fusion
  11.3 0.7 subtract_convert_fusion
  12.0 0.6 pad_maximum_fusion
  12.6 0.1 convert_element_type.81
  12.7 0.8 mul.225
  13.5 0.1 multiply_multiply_fusion.1
  13.6 0.2 subtract_convert_fusion.1
  13.8 0.2 pad_maximum_fusion.1
  14.0 33.0 %all_gather.12 = bf16[2048,128]{0,1:T(8,128)(2,1)S(1)} all-gather(bf16[256,128]{0,1:T(8,128)(2,1)S(1)} %convert_element_type.79), channel_id=1, replica_groups=mesh['sp'=8,'tp'=4] {'sp'}, dimensions={0}, use_global_device_ids=true | all-gather | bytes 589824 | tf_op jit(solution)/shard_map/all_gather | solution.py:78
  47.0 8.1 %bitcast_reduce_fusion = (f32[2,4,256]{2,1,0:T(4,128)S(1)}, f32[2,2048,256,4]{2,1,3,0:T(8,128)}) fusion(bf16[2048,2,64,1]{0,2,3,1:T(8,128)(2,1)S(1)} %bitcast.63, bf16[256,2,4,64]{0,3,2,1:T(8,128)(2,1)S(1)} %convert_element_type.81), kind=kOutput, calls=%fused_computation.1 | convolution fusion | flops 545257472 | bytes 17571840 | tf_op jit(solution)/shard_map/while/body/eval_jaxpr/qhgd,khd->hgqk/dot_general | solution.py:43
  55.1 0.0 copy-start.1
  55.1 8.5 %fusion.1 = f32[2,4,256]{2,1,0:T(4,128)S(1)} fusion(f32[2,2048,256,4]{2,1,3,0:T(8,128)} %get-tuple-element.42, f32[2,4,256]{2,1,0:T(4,128)S(1)} %get-tuple-element.38), kind=kLoop, calls=%fused_computation.3 | loop fusion | flops 12580864 | bytes 16793600 | tf_op jit(solution)/shard_map/while/body/eval_jaxpr/reduce_sum | solution.py:48
  63.7 0.0 copy-done.1
  63.7 31.3 %all_gather.13 = bf16[2048,128]{1,0:T(8,128)(2,1)S(1)} all-gather(bf16[256,128]{1,0:T(8,128)(2,1)S(1)} %copy-done.1), channel_id=1, replica_groups=mesh['sp'=8,'tp'=4] {'sp'}, dimensions={0}, use_global_device_ids=true | all-gather | bytes 589824 | tf_op jit(solution)/shard_map/all_gather | solution.py:79
  95.0 0.2 copy.19
  95.2 7.4 %fusion.22 = bf16[256,2,4,64]{0,3,2,1:T(8,128)(2,1)S(1)} fusion(bf16[2048,2,64,1]{0,2,3,1:T(8,128)(2,1)S(1)} %bitcast.62, f32[2,2048,256,4]{2,1,3,0:T(8,128)} %get-tuple-element.42, f32[2,4,256]{2,1,0:T(4,128)S(1)} %get-tuple-element.38, f32[256,2,4]{0,2,1:T(4,128)S(1)} %bitcast_add_fusion, f32[256,2,4]{0,2,1:T(4,128)S(1)} %get-tuple-element.37), kind=kOutput, calls=%fused_computation.22 | convolution fusion | flops 549847040 | bytes 17588224 | tf_op jit(solution)/shard_map/while/body/eval_jaxpr/hgqk,khd->hgqd/dot_general | solution.py:49
  102.6 0.0 copy-start.2
  102.6 0.0 copy-done
  102.6 1.8 convolution_convert_fusion
  104.3 0.0 all-reduce.2.cloned.1.call-update
  104.4 0.0 all-gather.3.cloned.1.call-start
  104.4 0.5 all-gather.3.cloned.1.call-update
  104.9 0.0 all-gather.5.cloned.1.call-start
  105.0 0.5 all-gather.5.cloned.1.call-update
  105.5 0.2 reduce-scatter.2.cloned.1.call-start
  105.8 36.5 %all-reduce.2.cloned.1.call-done = bf16[256,2048]{1,0:T(8,128)(2,1)} async-done(((bf16[256,2048]{1,0:T(8,128)(2,1)}), bf16[256,2048]{1,0:T(8,128)(2,1)}) %all-reduce.2.cloned.1.call-update) | async-done | bytes 1048592 | tf_op jit(solution)/shard_map/psum | solution.py:95
  142.3 2.1 fusion.7
  144.4 88.0 %all-gather.3.cloned.1.call-done = bf16[2048,2048]{1,0:T(8,128)(2,1)} async-done(((bf16[256,2048]{1,0:T(8,128)(2,1)}), bf16[2048,2048]{1,0:T(8,128)(2,1)}) %all-gather.3.cloned.1.call-update) | async-done | bytes 8388624 | tf_op jit(solution)/shard_map/all_gather | solution.py:107
  232.4 124.8 %all-gather.5.cloned.1.call-done = bf16[2048,2048]{1,0:T(8,128)(2,1)} async-done(((bf16[2048,256]{1,0:T(8,128)(2,1)}), bf16[2048,2048]{1,0:T(8,128)(2,1)}) %all-gather.5.cloned.1.call-update) | async-done | bytes 8388624 | tf_op jit(solution)/shard_map/all_gather | solution.py:113
  357.2 0.0 copy-done.2
  357.2 11.3 %convolution_convert_fusion.1 = bf16[256,2048]{1,0:T(8,128)(2,1)} fusion(bf16[2048,2048]{1,0:T(8,128)(2,1)} %all-gather.5.cloned.1.call-done, bf16[2048,2048]{1,0:T(8,128)(2,1)} %all-gather.3.cloned.1.call-done, bf16[256,2048]{1,0:T(8,128)(2,1)S(1)} %get-tuple-element.20, f32[2048]{0:T(1024)S(1)} %copy-done.2, f32[256]{0:T(256)S(1)} %add_rsqrt_fusion.2), kind=kOutput, calls=%fused_computation.12 | convolution fusion | flops 4299161600 | bytes 18883584 | tf_op jit(solution)/shard_map/dot_general | solution.py:111
  368.5 0.0 reduce-scatter.2.cloned.1.call-update
  368.5 23.1 %reduce-scatter.2.cloned.1.call-done = bf16[256,512]{1,0:T(8,128)(2,1)} async-done(((bf16[256,2048]{1,0:T(8,128)(2,1)}), bf16[256,512]{1,0:T(8,128)(2,1)}) %reduce-scatter.2.cloned.1.call-update) | async-done | bytes 262160 | tf_op jit(solution)/shard_map/reduce_scatter | solution.py:116
  391.6 1.7 add_convert_fusion.1
  (9 shorter events, 0.1 us)
Async XLA Ops:
  7.4 95.2 %copy-start = (bf16[512,2048]{1,0:T(8,128)(2,1)S(1)}, bf16[512,2048]{1,0:T(8,128)(2,1)}, u32[]{:S(2)}) copy-start(bf16[512,2048]{1,0:T(8,128)(2,1)} %param.16) | copy-start | bytes 6291460
  7.4 134.9 %all-reduce.2.cloned.1.call-start = ((), (), s32[]{:S(2)}) async-start(), calls=%async_computation.1 | async-start | bytes 2097152 | tf_op jit(solution)/shard_map/psum | solution.py:95
  55.1 8.6 %copy-start.1 = (bf16[256,128]{1,0:T(8,128)(2,1)S(1)}, bf16[256,128]{1,0:T(8,128)(2,1)}, u32[]{:S(2)}) copy-start(bf16[256,128]{1,0:T(8,128)(2,1)} %param.12) | copy-start | bytes 196612
  102.6 254.6 %copy-start.2 = (f32[2048]{0:T(1024)S(1)}, f32[2048]{0:T(1024)}, u32[]{:S(2)}) copy-start(f32[2048]{0:T(1024)} %param.17) | copy-start | bytes 24580
  104.4 128.0 %all-gather.3.cloned.1.call-start = ((), (), s32[]{:S(2)}) async-start(), calls=%async_computation.2 | async-start | bytes 9437184 | tf_op jit(solution)/shard_map/all_gather | solution.py:107
  104.9 252.3 %all-gather.5.cloned.1.call-start = ((), (), s32[]{:S(2)}) async-start(), calls=%async_computation.3 | async-start | bytes 9437184 | tf_op jit(solution)/shard_map/all_gather | solution.py:113
  105.5 286.1 %reduce-scatter.2.cloned.1.call-start = ((), (), s32[]{:S(2)}) async-start(), calls=%async_computation.4 | async-start | bytes 1310720 | tf_op jit(solution)/shard_map/reduce_scatter | solution.py:116
Sparse Core Ops, SparseCore 0:
  104.5 37.7 all-reduce.1
  368.6 22.9 reduce-scatter.1
Sparse Core Ops, SparseCore 1:
  107.0 125.3 all-gather.2
  234.3 122.9 all-gather.4
where the time goes:
time: 401 us
  waiting for transfers between devices  274 us (68%)
  blocking collectives  64.3 us (16%)
  matrix products  28.5 us (7%)
  between operations  15.1 us (4%)
  other arithmetic  14.7 us (4%)
  local copies, waits for them, and re-layouts  4.36 us (1%)
    all_gather x1, waiting for transfers between devices, shards(): lax.all_gather(down_weight, 'sp', axis=1, tiled=True)  125 us
    all_gather x1, waiting for transfers between devices, shards(): lax.all_gather(up_weight, 'sp', axis=0, tiled=True)  88 us
    psum x1, waiting for transfers between devices, shards(): lax.psum(partial_value.astype(jnp.bfloat16), 'tp').astype(jnp.float32)  36.5 us
    all_gather x1, blocking collectives, shards(): key_rows = lax.all_gather(prepared_keys, 'sp', axis=0, tiled=True)  33 us
    all_gather x1, blocking collectives, shards(): value_rows = lax.all_gather(values, 'sp', axis=0, tiled=True)  31.3 us
    reduce_scatter x1, waiting for transfers between devices, shards(): lax.psum_scatter(down_part.astype(jnp.bfloat16), 'tp', scatter_dimension=...  23.1 us
    dot_general x1, matrix products, shards(): jnp.dot(hidden, lax.all_gather(down_weight, 'sp', axis=1, tiled=True), pr...  11.3 us
    reduce_sum x1, other arithmetic, attend_block(): totals = totals * rescale + jnp.sum(exps, axis=-1)  8.52 us
  transfers between devices with their start and end apart: 4, of which 4 were waited for; matrix products, arithmetic and copies ran while one was open for 1% of the time, Pallas kernels for 0%

commit v1 on v0

--- a/solution.py
+++ b/solution.py
@@ -1,8 +1,11 @@
+import functools
 import math
 
 import jax
 import jax.numpy as jnp
 from jax import lax
+from jax.experimental import pallas as pl
+from jax.experimental.pallas import tpu as pltpu
 from jax.sharding import PartitionSpec as P
 
 HD = 64
@@ -119,9 +122,345 @@
     return (own_mid.astype(jnp.float32) + down_share).astype(jnp.bfloat16)
 
 
+def layer_kernel(
+    planes,
+    ranks,
+    q_ref,
+    kv_ref,
+    stream_ref,
+    out_w_ref,
+    gain_ref,
+    up_ref,
+    down_ref,
+    out_ref,
+    kv_all,
+    up_all,
+    down_all,
+    head_all,
+    first_send,
+    first_land,
+    pair_send,
+    pair_land,
+    mid_all,
+    core_send,
+    core_land,
+    core_keep,
+    x_send,
+    x_land,
+    z_send,
+    z_land,
+    send_sems,
+    recv_sems,
+):
+    rows = out_ref.shape[0]
+    cols = out_ref.shape[1]
+    lanes = q_ref.shape[2]
+    slab = up_ref.shape[1] // planes
+    depth = up_ref.shape[0]
+    own_sp = lax.axis_index("sp")
+    own_tp = lax.axis_index("tp")
+    plane, side = own_sp // 2, own_sp % 2
+    ex, core = own_tp // 2, own_tp % 2
+    y_peer = (plane * 2 + 1 - side, own_tp)
+    core_peer = (own_sp, ex * 2 + 1 - core)
+    x_peer = (own_sp, (1 - ex) * 2 + core)
+
+    def plane_at(offset):
+        return lax.rem(plane + offset + planes, planes)
+
+    def z_peer(offset):
+        return (plane_at(offset) * 2 + side, own_tp)
+
+    barrier = pltpu.get_barrier_semaphore()
+    greeted = [y_peer, core_peer, x_peer] + [z_peer(d) for d in range(1, planes)]
+    for peer in greeted:
+        pl.semaphore_signal(barrier, inc=1, device_id=peer, device_id_type=pl.DeviceIdType.MESH)
+    pl.semaphore_wait(barrier, len(greeted))
+
+    copies = []
+
+    def push(src, dst, peer):
+        slot = len(copies)
+        copy = pltpu.make_async_remote_copy(
+            src_ref=src,
+            dst_ref=dst,
+            send_sem=send_sems.at[slot],
+            recv_sem=recv_sems.at[slot],
+            device_id=peer,
+            device_id_type=pl.DeviceIdType.MESH,
+        )
+        copy.start()
+        copies.append(copy)
+        return copy
+
+    def kv_at(sp):
+        return kv_all.at[pl.ds(pl.multiple_of(sp * rows, rows), rows), :]
+
+    def up_at(sp):
+        return up_all.at[pl.ds(pl.multiple_of(sp * depth, depth), depth), :]
+
+    def down_at(sp):
+        return down_all.at[:, pl.ds(pl.multiple_of(sp * depth, depth), depth)]
+
+    def up_part(p):
+        return up_ref.at[:, pl.ds(pl.multiple_of(p * slab, slab), slab)]
+
+    def down_part(p):
+        return down_ref.at[pl.ds(pl.multiple_of(p * slab, slab), slab), :]
+
+    kv_z = {d: push(kv_ref, kv_at(own_sp), z_peer(d)) for d in range(1, planes)}
+    kv_y = {0: push(kv_ref, kv_at(own_sp), y_peer)}
+    up_z, down_z = {}, {}
+    for d in range(1, planes):
+        up_z[d] = push(up_part(plane_at(d)), up_at(own_sp), z_peer(d))
+        down_z[d] = push(down_part(plane_at(d)), down_at(own_sp), z_peer(d))
+    kv_at(own_sp)[...] = kv_ref[...]
+    up_at(own_sp)[...] = up_part(plane)[...]
+    down_at(own_sp)[...] = down_part(plane)[...]
+    for d in range(1, planes):
+        kv_z[d].wait_recv()
+        block = plane_at(-d) * 2 + side
+        kv_y[d] = push(kv_at(block), kv_at(block), y_peer)
+    up_y = {0: push(up_part(plane), up_at(own_sp), y_peer)}
+    down_y = {0: push(down_part(plane), down_at(own_sp), y_peer)}
+    for d in range(planes):
+        kv_y[d].wait_recv()
+
+    heads = q_ref.shape[0]
+    kv_heads = lanes // HD
+    pairs_each = heads // 2 // kv_heads
+
+    def attend(h):
+        scores = lax.dot_general(
+            q_ref[h],
+            kv_all[:, :lanes],
+            (((1,), (1,)), ((), ())),
+            preferred_element_type=jnp.float32,
+        )
+        exps = jnp.exp(scores - jnp.max(scores, axis=-1, keepdims=True))
+        totals = jnp.sum(exps, axis=-1, keepdims=True)
+        mixed = jnp.dot(
+            exps.astype(jnp.bfloat16), kv_all[:, lanes:], preferred_element_type=jnp.float32
+        )
+        return mixed / totals
+
+    def attend_pair(pair, carry):
+        first, second = attend(2 * pair), attend(2 * pair + 1)
+        low = pair < pairs_each
+        left = jnp.where(low, first, pltpu.roll(first, HD, 1))
+        right = jnp.where(low, pltpu.roll(second, HD, 1), second)
+        lane = lax.broadcasted_iota(jnp.int32, left.shape, 1)
+        head_all[pair] = jnp.where(lane < HD, left, right).astype(jnp.bfloat16)
+        return carry
+
+    lax.fori_loop(0, heads // 2, attend_pair, 0)
+
+    def columns(rank):
+        return pl.ds(pl.multiple_of(rank * cols, cols), cols)
+
+    def project(rank):
+        total = jnp.zeros((rows, cols), jnp.float32)
+        for pair in range(heads // 2):
+            total += jnp.dot(
+                head_all[pair],
+                out_w_ref[pair * lanes : (pair + 1) * lanes, columns(rank)],
+                preferred_element_type=jnp.float32,
+            )
+        return total.astype(jnp.bfloat16)
+
+    far, near = (1 - ex) * 2, ex * 2
+    first_send[0] = project(far + 1 - core)
+    pass_far = push(first_send.at[0], first_land.at[0], core_peer)
+    first_send[1] = project(near + 1 - core)
+    pass_near = push(first_send.at[1], first_land.at[1], core_peer)
+    far_own = project(far + core).astype(jnp.float32)
+    pass_far.wait_recv()
+    pair_send[...] = (far_own + first_land[0].astype(jnp.float32)).astype(jnp.bfloat16)
+    pass_x = push(pair_send, pair_land, x_peer)
+    near_own = project(near + core).astype(jnp.float32)
+    pass_near.wait_recv()
+    near_own += first_land[1].astype(jnp.float32)
+    near_own += stream_ref[:, columns(own_tp)].astype(jnp.float32)
+    pass_x.wait_recv()
+    mid = (near_own + pair_land[...].astype(jnp.float32)).astype(jnp.bfloat16)
+    mid_all[plane, own_tp] = mid
+
+    own_mid = mid_all.at[plane, own_tp]
+    mid_z = {d: push(own_mid, own_mid, z_peer(d)) for d in range(1, planes)}
+    mid_x = {0: push(own_mid, own_mid, x_peer)}
+    mid_c = {0: push(own_mid, own_mid, core_peer)}
+    mid_d = {}
+
+    for d in range(1, planes):
+        block = plane_at(-d) * 2 + side
+        up_z[d].wait_recv()
+        up_y[d] = push(up_at(block), up_at(block), y_peer)
+        down_z[d].wait_recv()
+        down_y[d] = push(down_at(block), down_at(block), y_peer)
+
+    core_far, core_near, x_pass, z_pass = {}, {}, {}, {}
+
+    def spread(d):
+        mid_z[d].wait_recv()
+        ref = mid_all.at[plane_at(-d), own_tp]
+        mid_x[d] = push(ref, ref, x_peer)
+        mid_c[d] = push(ref, ref, core_peer)
+
+    def mix(d):
+        where_z = plane_at(-d)
+        wide = [mid_all[where_z, r].astype(jnp.float32) for r in range(ranks)]
+        square = sum(jnp.sum(w * w, axis=-1, keepdims=True) for w in wide)
+        inverse = lax.rsqrt(square / (ranks * cols) + EPSILON)
+        sums = jnp.zeros((rows, slab), jnp.float32)
+        for r in range(ranks):
+            normed = wide[r] * inverse * gain_ref[:, r * cols : (r + 1) * cols]
+            sums += jnp.dot(
+                normed.astype(jnp.bfloat16),
+                up_all[r * cols : (r + 1) * cols, :],
+                preferred_element_type=jnp.float32,
+            )
+        return jnp.square(jnp.maximum(sums, 0.0)).astype(jnp.bfloat16)
+
+    def lower(hidden, rank):
+        part = jnp.dot(hidden, down_all[:, columns(rank)], preferred_element_type=jnp.float32)
+        return part.astype(jnp.bfloat16)
+
+    def core_stage(d):
+        hidden = mix(d)
+        core_send[d, 0] = lower(hidden, far + 1 - core)
+        core_far[d] = push(core_send.at[d, 0], core_land.at[d, 0], core_peer)
+        core_send[d, 1] = lower(hidden, near + 1 - core)
+        core_near[d] = push(core_send.at[d, 1], core_land.at[d, 1], core_peer)
+        core_keep[d, 0] = lower(hidden, far + core)
+        core_keep[d, 1] = lower(hidden, near + core)
+
+    def x_stage(d):
+        core_far[d].wait_recv()
+        x_send[d] = (
+            core_keep[d, 0].astype(jnp.float32) + core_land[d, 0].astype(jnp.float32)
+        ).astype(jnp.bfloat16)
+        x_pass[d] = push(x_send.at[d], x_land.at[d], x_peer)
+
+    def z_stage(d):
+        core_near[d].wait_recv()
+        x_pass[d].wait_recv()
+        total = core_keep[d, 1].astype(jnp.float32) + core_land[d, 1].astype(jnp.float32)
+        total += x_land[d].astype(jnp.float32)
+        z_send[d] = total.astype(jnp.bfloat16)
+        if d:
+            z_pass[d] = push(z_send.at[d], z_land.at[d], z_peer(-d))
+
+    for d in range(planes):
+        if d + 1 < planes:
+            spread(d + 1)
+        mid_x[d].wait_recv()
+        ref = mid_all.at[plane_at(-d), x_peer[1]]
+        mid_d[d] = push(ref, ref, core_peer)
+        if d == 0:
+            for e in range(planes):
+                up_y[e].wait_recv()
+                down_y[e].wait_recv()
+        mid_c[d].wait_recv()
+        mid_d[d].wait_recv()
+        core_stage(d)
+        if d >= 1:
+            x_stage(d - 1)
+        if d >= 2:
+            z_stage(d - 2)
+    x_stage(planes - 1)
+    for d in range(max(planes - 2, 0), planes):
+        z_stage(d)
+    total = mid_all[plane, own_tp].astype(jnp.float32) + z_send[0].astype(jnp.float32)
+    for d in range(1, planes):
+        z_pass[d].wait_recv()
+        total += z_land[d].astype(jnp.float32)
+    out_ref[...] = total.astype(jnp.bfloat16)
+    for copy in copies:
+        copy.wait_send()
+
+
+def fused_shards(
+    size_sp,
+    size_tp,
+    queries,
+    keys,
+    values,
+    query_gain,
+    key_gain,
+    stream,
+    out_weight,
+    mixer_gain,
+    up_weight,
+    down_weight,
+):
+    planes = size_sp // 2
+    rows, width = queries.shape
+    lanes = keys.shape[1]
+    heads = width // HD
+    group_size = heads // (lanes // HD)
+    cols = stream.shape[1] // size_tp
+    offset = lax.axis_index("sp") * rows
+    prepared_q = prepare(queries, query_gain, offset)
+    prepared_k = prepare(keys, key_gain, offset).reshape(rows, lanes)
+    prepared_q = jnp.transpose(prepared_q, (1, 0, 2)) * jnp.bfloat16(1.0 / math.sqrt(HD))
+    blank = jnp.zeros_like(prepared_q[:group_size])
+    padded = jnp.concatenate(
+        [
+            jnp.concatenate([prepared_q[:group_size], blank], axis=-1),
+            jnp.concatenate([blank, prepared_q[group_size:]], axis=-1),
+        ],
+        axis=0,
+    )
+    kv = jnp.concatenate([prepared_k, values], axis=1)
+    slab = up_weight.shape[1] // planes
+    half = jnp.bfloat16
+    tile = (rows, cols)
+    total_copies = 64
+    vmem = pl.BlockSpec(memory_space=pltpu.VMEM)
+    scratch = [
+        pltpu.VMEM((size_sp * rows, 2 * lanes), half),
+        pltpu.VMEM((stream.shape[1], slab), half),
+        pltpu.VMEM((slab, stream.shape[1]), half),
+        pltpu.VMEM((heads // 2, rows, lanes), half),
+        pltpu.VMEM((2,) + tile, half),
+        pltpu.VMEM((2,) + tile, half),
+        pltpu.VMEM(tile, half),
+        pltpu.VMEM(tile, half),
+        pltpu.VMEM((planes, size_tp) + tile, half),
+        pltpu.VMEM((planes, 2) + tile, half),
+        pltpu.VMEM((planes, 2) + tile, half),
+        pltpu.VMEM((planes, 2) + tile, half),
+        pltpu.VMEM((planes,) + tile, half),
+        pltpu.VMEM((planes,) + tile, half),
+        pltpu.VMEM((planes,) + tile, half),
+        pltpu.VMEM((planes,) + tile, half),
+        pltpu.SemaphoreType.DMA((total_copies,)),
+        pltpu.SemaphoreType.DMA((total_copies,)),
+    ]
+    return pl.pallas_call(
+        functools.partial(layer_kernel, planes, size_tp),
+        out_shape=jax.ShapeDtypeStruct(tile, half),
+        in_specs=[vmem] * 7,
+        out_specs=vmem,
+        scratch_shapes=scratch,
+        compiler_params=pltpu.CompilerParams(
+            collective_id=0, has_side_effects=True, vmem_limit_bytes=60 * 2**20
+        ),
+        name="layer",
+    )(padded, kv, stream, out_weight, mixer_gain[None, :], up_weight, down_weight)
+
+
 def solution(mesh):
+    size_sp, size_tp = mesh.shape["sp"], mesh.shape["tp"]
+
+    def body(*arrays):
+        tiled = arrays[9].shape[1] % 128 == 0 and arrays[1].shape[1] == 2 * HD
+        if tiled and size_tp == 4 and size_sp % 2 == 0:
+            return fused_shards(size_sp, size_tp, *arrays)
+        return shards(*arrays)
+
     return jax.shard_map(
-        shards,
+        body,
         mesh=mesh,
         in_specs=(
             P("sp", "tp"),

time: 401 us -> 155 us (0.39)
  the two profiles are of different devices: /device:TPU:0 before, /device:TPU:17 now
where the time goes in v1:
time: 155 us
  Pallas kernels  146 us (94%)
  local copies, waits for them, and re-layouts  4.77 us (3%)
  other arithmetic  3.97 us (3%)
    pallas_call x1, Pallas kernels, fused_shards(): pl.pallas_call(functools.partial(layer_kernel, planes, size_tp), out_shap...  146 us

profile of v1, /device:TPU:17, one launch (start us, length us, event | category | flops | bytes accessed | tf_op | source)
XLA Modules:
  0.0 154.7 jit_solution(7242721386118860866)
XLA Ops:
  0.0 0.1 broadcast_multiply_fusion.1
  0.1 0.1 fusion.4
  0.2 1.1 copy.12
  1.3 0.3 reshape.136
  1.6 0.1 bitcast_reduce_fusion
  1.7 0.8 mul.184
  2.4 0.3 multiply_multiply_fusion
  2.7 0.7 subtract_convert_fusion
  3.4 0.0 copy-start
  3.4 0.6 maximum_multiply_fusion
  4.0 0.0 copy-start.2
  4.1 0.2 copy.13
  4.3 0.0 copy-start.1
  4.3 0.3 copy.14
  4.7 0.9 fusion.2.q_ref
  5.6 0.0 copy-done
  5.6 0.1 copy.15
  5.7 0.1 reshape.137
  5.8 0.0 copy-done.2
  5.8 0.1 mul.207
  6.0 0.1 multiply_multiply_fusion.1
  6.1 0.2 subtract_convert_fusion.1
  6.3 0.2 pad_maximum_fusion.1
  6.5 0.1 copy.16
  6.6 0.0 copy-done.1
  6.6 0.7 pad_maximum_fusion.kv_ref
  7.3 145.7 %layer.1 = bf16[256,512]{1,0:T(8,128)(2,1)} custom-call(bf16[8,256,128]{2,1,0:T(8,128)(2,1)} %fusion.2.q_ref, bf16[256,256]{1,0:T(8,128)(2,1)} %pad_maximum_fusion.kv_ref, bf16[256,2048]{1,0:T(8,128)(2,1)} %stream_ref.1, bf16[512,2048]{1,0:T(8,128)(2,1)} %out_w_ref.1, f32[1,2048]{1,0:T(1,128)} %bitcast.15, bf16[256,2048]{1,0:T(8,128)(2,1)} %up_ref.1, ...), custom_call_target="tpu_custom_call" | custom-call | tf_op jit(solution)/shard_map/layer/pallas_call | solution.py:440
  153.0 1.7 %copy.18 = bf16[256,512]{1,0:T(8,128)(2,1)} copy(bf16[256,512]{1,0:T(8,128)(2,1)} %layer.1) | data formatting | bytes 524288
  (7 shorter events, 0.1 us)
Async XLA Ops:
  3.4 2.2 %copy-start = (bf16[256,128]{1,0:T(8,128)(2,1)S(1)}, bf16[256,128]{1,0:T(8,128)(2,1)}, u32[]{:S(2)}) copy-start(bf16[256,128]{1,0:T(8,128)(2,1)} %param.11) | copy-start | bytes 196612
  4.0 1.8 %copy-start.2 = (f32[64]{0:T(128)S(1)}, f32[64]{0:T(128)}, u32[]{:S(2)}) copy-start(f32[64]{0:T(128)} %param.14) | copy-start | bytes 772
  4.3 2.3 %copy-start.1 = (bf16[256,128]{1,0:T(8,128)(2,1)S(1)}, bf16[256,128]{1,0:T(8,128)(2,1)}, u32[]{:S(2)}) copy-start(bf16[256,128]{1,0:T(8,128)(2,1)} %param.12) | copy-start | bytes 196612

commit v2 on v1

--- a/solution.py
+++ b/solution.py
@@ -126,13 +126,17 @@
     planes,
     ranks,
     q_ref,
-    kv_ref,
+    k_ref,
+    v_ref,
+    tables_ref,
+    gains_ref,
     stream_ref,
     out_w_ref,
     gain_ref,
     up_ref,
     down_ref,
     out_ref,
+    q_all,
     kv_all,
     up_all,
     down_all,
@@ -154,7 +158,7 @@
 ):
     rows = out_ref.shape[0]
     cols = out_ref.shape[1]
-    lanes = q_ref.shape[2]
+    lanes = q_all.shape[2]
     slab = up_ref.shape[1] // planes
     depth = up_ref.shape[0]
     own_sp = lax.axis_index("sp")
@@ -171,6 +175,13 @@
     def z_peer(offset):
         return (plane_at(offset) * 2 + side, own_tp)
 
+    def nearest(place):
+        found = 0
+        for p in range(planes):
+            ranked = sorted(range(planes), key=lambda b: (abs(b - p), b if 2 * p < planes else -b))
+            found = found + jnp.where(plane == p, ranked[place], 0)
+        return found
+
     barrier = pltpu.get_barrier_semaphore()
     greeted = [y_peer, core_peer, x_peer] + [z_peer(d) for d in range(1, planes)]
     for peer in greeted:
@@ -179,8 +190,14 @@
 
     copies = []
 
+    slots = [0]
+
+    def take(count):
+        slots[0] += count
+        return slots[0] - count
+
     def push(src, dst, peer):
-        slot = len(copies)
+        slot = take(1)
         copy = pltpu.make_async_remote_copy(
             src_ref=src,
             dst_ref=dst,
@@ -193,6 +210,41 @@
         copies.append(copy)
         return copy
 
+    guarded = []
+
+    def line(ref_of):
+        base = take(planes + 2)
+
+        def copy_of(b, send_slot, step):
+            ref = ref_of(b)
+            return pltpu.make_async_remote_copy(
+                src_ref=ref,
+                dst_ref=ref,
+                send_sem=send_sems.at[send_slot],
+                recv_sem=recv_sems.at[base + b],
+                device_id=(jnp.clip(plane + step, 0, planes - 1) * 2 + side, own_tp),
+                device_id_type=pl.DeviceIdType.MESH,
+            )
+
+        def begin(b, send_slot, step, valid):
+            copy = copy_of(b, send_slot, step)
+            pl.when(valid)(copy.start)
+            guarded.append((valid, copy))
+
+        def start(src=None):
+            for slot, step, valid in (
+                (planes, 1, plane < planes - 1),
+                (planes + 1, -1, plane > 0),
+            ):
+                begin(plane, base + slot, step, valid)
+
+        def arrive(b):
+            copy_of(b, base + b, 1).wait_recv()
+            begin(b, base + b, 1, jnp.logical_and(b < plane, plane < planes - 1))
+            begin(b, base + b, -1, jnp.logical_and(b > plane, plane > 0))
+
+        return start, arrive
+
     def kv_at(sp):
         return kv_all.at[pl.ds(pl.multiple_of(sp * rows, rows), rows), :]
 
@@ -208,31 +260,69 @@
     def down_part(p):
         return down_ref.at[pl.ds(pl.multiple_of(p * slab, slab), slab), :]
 
-    kv_z = {d: push(kv_ref, kv_at(own_sp), z_peer(d)) for d in range(1, planes)}
-    kv_y = {0: push(kv_ref, kv_at(own_sp), y_peer)}
+    cosine, signed_sine = tables_ref[0], tables_ref[1]
+    lane = lax.broadcasted_iota(jnp.int32, (rows, lanes), 1)
+    is_low, is_even = lane < HD, lane % 2 == 0
+
+    def turned(block, gain):
+        wide = block.astype(jnp.float32)
+        square = wide * wide
+        low = jnp.sum(jnp.where(is_low, square, 0.0), axis=-1, keepdims=True)
+        high = jnp.sum(jnp.where(is_low, 0.0, square), axis=-1, keepdims=True)
+        wide = wide * lax.rsqrt(jnp.where(is_low, low, high) / HD + EPSILON) * gain
+        partner = jnp.where(is_even, pltpu.roll(wide, lanes - 1, 1), pltpu.roll(wide, 1, 1))
+        return (wide * cosine + partner * signed_sine).astype(jnp.bfloat16)
+
+    own_rows = pl.ds(pl.multiple_of(own_sp * rows, rows), rows)
+    kv_all[own_rows, :lanes] = turned(k_ref[...], gains_ref[1:2])
+    kv_all[own_rows, lanes:] = v_ref[...]
+    kv_start, kv_arrive = line(lambda b: kv_at(b * 2 + side))
+    kv_start()
+    kv_y = {0: push(kv_at(own_sp), kv_at(own_sp), y_peer)}
     up_z, down_z = {}, {}
-    for d in range(1, planes):
+    offsets = sorted(range(1, planes), key=lambda d: (d != planes // 2, d))
+    for d in offsets:
         up_z[d] = push(up_part(plane_at(d)), up_at(own_sp), z_peer(d))
+    for d in offsets:
         down_z[d] = push(down_part(plane_at(d)), down_at(own_sp), z_peer(d))
-    kv_at(own_sp)[...] = kv_ref[...]
     up_at(own_sp)[...] = up_part(plane)[...]
     down_at(own_sp)[...] = down_part(plane)[...]
+    blocks = q_ref.shape[1] // lanes
+    for i in range(blocks):
+        block = turned(q_ref[:, i * lanes : (i + 1) * lanes], gains_ref[0:1]).astype(jnp.float32)
+        block = block * (1.0 / math.sqrt(HD))
+        swapped = pltpu.roll(block, HD, 1)
+        low = 2 * i < blocks
+        mine = is_low if low else jnp.logical_not(is_low)
+        pair = (block, swapped) if low else (swapped, block)
+        for h in range(2):
+            q_all[2 * i + h] = jnp.where(mine, pair[h], 0.0).astype(jnp.bfloat16)
     for d in range(1, planes):
-        kv_z[d].wait_recv()
-        block = plane_at(-d) * 2 + side
-        kv_y[d] = push(kv_at(block), kv_at(block), y_peer)
+        b = nearest(d)
+        kv_arrive(b)
+        kv_y[d] = push(kv_at(b * 2 + side), kv_at(b * 2 + side), y_peer)
     up_y = {0: push(up_part(plane), up_at(own_sp), y_peer)}
     down_y = {0: push(down_part(plane), down_at(own_sp), y_peer)}
     for d in range(planes):
         kv_y[d].wait_recv()
 
-    heads = q_ref.shape[0]
+    def forward_up(d):
+        block = plane_at(-d) * 2 + side
+        up_z[d].wait_recv()
+        up_y[d] = push(up_at(block), up_at(block), y_peer)
+
+    def forward_down(d):
+        block = plane_at(-d) * 2 + side
+        down_z[d].wait_recv()
+        down_y[d] = push(down_at(block), down_at(block), y_peer)
+
+    heads = q_all.shape[0]
     kv_heads = lanes // HD
     pairs_each = heads // 2 // kv_heads
 
     def attend(h):
         scores = lax.dot_general(
-            q_ref[h],
+            q_all[h],
             kv_all[:, :lanes],
             (((1,), (1,)), ((), ())),
             preferred_element_type=jnp.float32,
@@ -254,6 +344,7 @@
         return carry
 
     lax.fori_loop(0, heads // 2, attend_pair, 0)
+    forward_up(offsets[0])
 
     def columns(rank):
         return pl.ds(pl.multiple_of(rank * cols, cols), cols)
@@ -286,28 +377,38 @@
     mid_all[plane, own_tp] = mid
 
     own_mid = mid_all.at[plane, own_tp]
-    mid_z = {d: push(own_mid, own_mid, z_peer(d)) for d in range(1, planes)}
+    mid_start, mid_arrive = line(lambda b: mid_all.at[b, own_tp])
+    mid_start()
     mid_x = {0: push(own_mid, own_mid, x_peer)}
     mid_c = {0: push(own_mid, own_mid, core_peer)}
     mid_d = {}
-
-    for d in range(1, planes):
-        block = plane_at(-d) * 2 + side
-        up_z[d].wait_recv()
-        up_y[d] = push(up_at(block), up_at(block), y_peer)
-        down_z[d].wait_recv()
-        down_y[d] = push(down_at(block), down_at(block), y_peer)
+    for d in offsets[1:]:
+        forward_up(d)
+    for d in offsets:
+        forward_down(d)
 
     core_far, core_near, x_pass, z_pass = {}, {}, {}, {}
 
     def spread(d):
-        mid_z[d].wait_recv()
-        ref = mid_all.at[plane_at(-d), own_tp]
+        mid_arrive(nearest(d))
+        ref = mid_all.at[nearest(d), own_tp]
         mid_x[d] = push(ref, ref, x_peer)
         mid_c[d] = push(ref, ref, core_peer)
 
+    z_base = take(planes)
+
+    def z_copy(d, target, sender):
+        return pltpu.make_async_remote_copy(
+            src_ref=z_send.at[d],
+            dst_ref=z_land.at[sender],
+            send_sem=send_sems.at[z_base + d],
+            recv_sem=recv_sems.at[z_base + sender],
+            device_id=(target * 2 + side, own_tp),
+            device_id_type=pl.DeviceIdType.MESH,
+        )
+
     def mix(d):
-        where_z = plane_at(-d)
+        where_z = nearest(d)
         wide = [mid_all[where_z, r].astype(jnp.float32) for r in range(ranks)]
         square = sum(jnp.sum(w * w, axis=-1, keepdims=True) for w in wide)
         inverse = lax.rsqrt(square / (ranks * cols) + EPSILON)
@@ -348,13 +449,15 @@
         total += x_land[d].astype(jnp.float32)
         z_send[d] = total.astype(jnp.bfloat16)
         if d:
-            z_pass[d] = push(z_send.at[d], z_land.at[d], z_peer(-d))
+            z_pass[d] = z_copy(d, nearest(d), plane)
+            z_pass[d].start()
+            copies.append(z_pass[d])
 
     for d in range(planes):
         if d + 1 < planes:
             spread(d + 1)
         mid_x[d].wait_recv()
-        ref = mid_all.at[plane_at(-d), x_peer[1]]
+        ref = mid_all.at[nearest(d), x_peer[1]]
         mid_d[d] = push(ref, ref, core_peer)
         if d == 0:
             for e in range(planes):
@@ -372,11 +475,14 @@
         z_stage(d)
     total = mid_all[plane, own_tp].astype(jnp.float32) + z_send[0].astype(jnp.float32)
     for d in range(1, planes):
-        z_pass[d].wait_recv()
-        total += z_land[d].astype(jnp.float32)
+        sender = nearest(d)
+        z_copy(d, sender, sender).wait_recv()
+        total += z_land[sender].astype(jnp.float32)
     out_ref[...] = total.astype(jnp.bfloat16)
     for copy in copies:
         copy.wait_send()
+    for valid, copy in guarded:
+        pl.when(valid)(copy.wait_send)
 
 
 def fused_shards(
@@ -397,27 +503,25 @@
     rows, width = queries.shape
     lanes = keys.shape[1]
     heads = width // HD
-    group_size = heads // (lanes // HD)
     cols = stream.shape[1] // size_tp
-    offset = lax.axis_index("sp") * rows
-    prepared_q = prepare(queries, query_gain, offset)
-    prepared_k = prepare(keys, key_gain, offset).reshape(rows, lanes)
-    prepared_q = jnp.transpose(prepared_q, (1, 0, 2)) * jnp.bfloat16(1.0 / math.sqrt(HD))
-    blank = jnp.zeros_like(prepared_q[:group_size])
-    padded = jnp.concatenate(
-        [
-            jnp.concatenate([prepared_q[:group_size], blank], axis=-1),
-            jnp.concatenate([blank, prepared_q[group_size:]], axis=-1),
-        ],
-        axis=0,
-    )
-    kv = jnp.concatenate([prepared_k, values], axis=1)
+    position = lax.axis_index("sp") * rows + jnp.arange(rows, dtype=jnp.int32)
+    grid_row = (position // GRID_W).astype(jnp.float32)[:, None]
+    grid_col = (position % GRID_W).astype(jnp.float32)[:, None]
+    lane = jnp.arange(lanes, dtype=jnp.int32)
+    pair = lane % HD // 2
+    quarter = HD // 4
+    inverse = 1.0 / jnp.power(10000.0, (pair % quarter * 2).astype(jnp.float32) / (HD // 2))
+    angle = jnp.where(pair < quarter, grid_row, grid_col) * inverse
+    sine = jnp.sin(angle)
+    tables = jnp.stack([jnp.cos(angle), jnp.where(lane % 2 == 0, -sine, sine)])
+    gains = jnp.stack([jnp.tile(query_gain, lanes // HD), jnp.tile(key_gain, lanes // HD)])
     slab = up_weight.shape[1] // planes
     half = jnp.bfloat16
     tile = (rows, cols)
-    total_copies = 64
+    total_copies = 96
     vmem = pl.BlockSpec(memory_space=pltpu.VMEM)
     scratch = [
+        pltpu.VMEM((heads, rows, lanes), half),
         pltpu.VMEM((size_sp * rows, 2 * lanes), half),
         pltpu.VMEM((stream.shape[1], slab), half),
         pltpu.VMEM((slab, stream.shape[1]), half),
@@ -440,14 +544,14 @@
     return pl.pallas_call(
         functools.partial(layer_kernel, planes, size_tp),
         out_shape=jax.ShapeDtypeStruct(tile, half),
-        in_specs=[vmem] * 7,
+        in_specs=[vmem] * 10,
         out_specs=vmem,
         scratch_shapes=scratch,
         compiler_params=pltpu.CompilerParams(
             collective_id=0, has_side_effects=True, vmem_limit_bytes=60 * 2**20
         ),
         name="layer",
-    )(padded, kv, stream, out_weight, mixer_gain[None, :], up_weight, down_weight)
+    )(queries, keys, values, tables, gains, stream, out_weight, mixer_gain[None, :], up_weight, down_weight)
 
 
 def solution(mesh):

time: 155 us -> 176 us (1.14)
  the two profiles are of different devices: /device:TPU:17 before, /device:TPU:0 now
where the time goes in v2:
time: 176 us
  Pallas kernels  171 us (97%)
  local copies, waits for them, and re-layouts  3.15 us (2%)
  other arithmetic  1.91 us (1%)
    pallas_call x1, Pallas kernels, fused_shards(): pl.pallas_call(functools.partial(layer_kernel, planes, size_tp), out_shap...  171 us

profile of v2, /device:TPU:0, one launch (start us, length us, event | category | flops | bytes accessed | tf_op | source)
XLA Modules:
  0.0 176.1 jit_solution(11170954741036073974)
XLA Ops:
  0.0 0.7 tile.4
  0.7 0.1 stack_tile.6
  0.8 0.7 tile.5
  1.4 0.1 stack_tile.7
  1.5 0.6 pad_maximum_fusion.1.gains_ref
  2.1 0.6 fusion
  2.7 0.7 pad_maximum_fusion.tables_ref
  3.4 171.0 %layer.1 = bf16[256,512]{1,0:T(8,128)(2,1)} custom-call(bf16[256,512]{1,0:T(8,128)(2,1)} %q_ref.1, bf16[256,128]{1,0:T(8,128)(2,1)} %k_ref.1, bf16[256,128]{1,0:T(8,128)(2,1)} %v_ref.1, f32[2,256,128]{2,1,0:T(8,128)} %pad_maximum_fusion.tables_ref, f32[2,128]{1,0:T(2,128)} %pad_maximum_fusion.1.gains_ref, bf16[256,2048]{1,0:T(8,128)(2,1)} %stream_ref.1, ...), custom_call_target="tpu_custom_call" | custom-call | tf_op jit(solution)/shard_map/layer/pallas_call | solution.py:544
  174.4 1.7 copy.12
  (3 shorter events, 0.0 us)

commit v3 on v2

--- a/solution.py
+++ b/solution.py
@@ -212,8 +212,22 @@
 
     guarded = []
 
-    def line(ref_of):
+    def line(ref_of, relay):
         base = take(planes + 2)
+
+        def straight():
+            ref = ref_of(plane)
+            for place in range(1, planes):
+                copy = pltpu.make_async_remote_copy(
+                    src_ref=ref,
+                    dst_ref=ref,
+                    send_sem=send_sems.at[base + place],
+                    recv_sem=recv_sems.at[base + plane],
+                    device_id=(nearest(place) * 2 + side, own_tp),
+                    device_id_type=pl.DeviceIdType.MESH,
+                )
+                copy.start()
+                copies.append(copy)
 
         def copy_of(b, send_slot, step):
             ref = ref_of(b)
@@ -231,7 +245,9 @@
             pl.when(valid)(copy.start)
             guarded.append((valid, copy))
 
-        def start(src=None):
+        def start():
+            if not relay:
+                return straight()
             for slot, step, valid in (
                 (planes, 1, plane < planes - 1),
                 (planes + 1, -1, plane > 0),
@@ -240,6 +256,8 @@
 
         def arrive(b):
             copy_of(b, base + b, 1).wait_recv()
+            if not relay:
+                return
             begin(b, base + b, 1, jnp.logical_and(b < plane, plane < planes - 1))
             begin(b, base + b, -1, jnp.logical_and(b > plane, plane > 0))
 
@@ -276,7 +294,7 @@
     own_rows = pl.ds(pl.multiple_of(own_sp * rows, rows), rows)
     kv_all[own_rows, :lanes] = turned(k_ref[...], gains_ref[1:2])
     kv_all[own_rows, lanes:] = v_ref[...]
-    kv_start, kv_arrive = line(lambda b: kv_at(b * 2 + side))
+    kv_start, kv_arrive = line(lambda b: kv_at(b * 2 + side), False)
     kv_start()
     kv_y = {0: push(kv_at(own_sp), kv_at(own_sp), y_peer)}
     up_z, down_z = {}, {}
@@ -377,7 +395,7 @@
     mid_all[plane, own_tp] = mid
 
     own_mid = mid_all.at[plane, own_tp]
-    mid_start, mid_arrive = line(lambda b: mid_all.at[b, own_tp])
+    mid_start, mid_arrive = line(lambda b: mid_all.at[b, own_tp], True)
     mid_start()
     mid_x = {0: push(own_mid, own_mid, x_peer)}
     mid_c = {0: push(own_mid, own_mid, core_peer)}

time: 176 us -> 147 us (0.84)
  Pallas kernels: 171 us -> 141 us
    pallas_call x1, Pallas kernels: 171 us -> 141 us  [fused_shards(): pl.pallas_call(functools.partial(layer_kernel, planes, size_tp), out_shap...]
where the time goes in v3:
time: 147 us; the launch traced here: 146 us
  Pallas kernels  141 us (96%)
  local copies, waits for them, and re-layouts  3.15 us (2%)
  other arithmetic  1.91 us (1%)
    pallas_call x1, Pallas kernels, fused_shards(): pl.pallas_call(functools.partial(layer_kernel, planes, size_tp), out_shap...  141 us

profile of v3, /device:TPU:0, one launch (start us, length us, event | category | flops | bytes accessed | tf_op | source)
XLA Modules:
  0.0 146.4 jit_solution(16370873093077946896)
XLA Ops:
  0.0 0.7 tile.4
  0.7 0.1 stack_tile.6
  0.8 0.7 tile.5
  1.4 0.1 stack_tile.7
  1.5 0.6 pad_maximum_fusion.1.gains_ref
  2.1 0.6 fusion
  2.7 0.7 pad_maximum_fusion.tables_ref
  3.4 141.3 %layer.1 = bf16[256,512]{1,0:T(8,128)(2,1)} custom-call(bf16[256,512]{1,0:T(8,128)(2,1)} %q_ref.1, bf16[256,128]{1,0:T(8,128)(2,1)} %k_ref.1, bf16[256,128]{1,0:T(8,128)(2,1)} %v_ref.1, f32[2,256,128]{2,1,0:T(8,128)} %pad_maximum_fusion.tables_ref, f32[2,128]{1,0:T(2,128)} %pad_maximum_fusion.1.gains_ref, bf16[256,2048]{1,0:T(8,128)(2,1)} %stream_ref.1, ...), custom_call_target="tpu_custom_call" | custom-call | tf_op jit(solution)/shard_map/layer/pallas_call | solution.py:562
  144.7 1.7 %copy.12 = bf16[256,512]{1,0:T(8,128)(2,1)} copy(bf16[256,512]{1,0:T(8,128)(2,1)} %layer.1) | data formatting | bytes 524288
  (3 shorter events, 0.0 us)
